TPU v7x, 32 devices: a whole 2x2x4 slice. The times are simulated.
32 devices in a mesh: sp: 8 (over z, y), tp: 4 (over x, core).
Axes of the slice: x: 2, y: 2, z: 4, core: 2. Of those that a mesh axis runs over, the one named last changes fastest.
Arguments:
- queries_one: bfloat16 [2048, 512], P('sp', 'tp'), may hold values from -6 to 6
- queries_two: bfloat16 [2048, 512], P('sp', 'tp'), may hold values from -6 to 6
- keys_one: bfloat16 [2048, 512], P('sp', 'tp'), may hold values from -6 to 6
- keys_two: bfloat16 [2048, 512], P('sp', 'tp'), may hold values from -6 to 6
- values: bfloat16 [2048, 1024], P('sp', 'tp'), may hold values from -6 to 6
- mix_lambda: float32 [4], P('tp'), may hold values from 0.3 to 0.8
- head_gain: float32 [1024], P('tp'), may hold values from 0.1 to 1.9
- out_weight: bfloat16 [1024, 2048], P('tp'), may hold values from -0.1875 to 0.1875
- residual_in: bfloat16 [2048, 2048], P('sp', 'tp'), may hold values from -12 to 12
- norm_gain: float32 [2048], replicated, may hold values from 0.1 to 1.9
- gate_weight: bfloat16 [2048, 5632], P('sp', 'tp'), may hold values from -0.125 to 0.125
- up_weight: bfloat16 [2048, 5632], P('sp', 'tp'), may hold values from -0.125 to 0.125
- down_weight: bfloat16 [5632, 2048], P('tp', 'sp'), may hold values from -0.078125 to 0.078125
Outputs:
- layer_out: bfloat16 [2048, 2048], P('sp', 'tp')
All inputs are finite; a program needn't handle non-finite values.
Results may differ from a plain program's by a relative error of at most 0.012.
Values may be sent and summed in bfloat16 or wider, within the bound.
A program may use at most 192 MiB of HBM per device.

v0:
```python
import jax
import jax.numpy as jnp
from jax import lax
from jax.sharding import PartitionSpec as P

HEAD = 128
epsilon = 1e-06
masked_score = -1e30


def per_device(
    queries_one,
    queries_two,
    keys_one,
    keys_two,
    values,
    mix_lambda,
    head_gain,
    out_weight,
    residual_in,
    norm_gain,
    gate_weight,
    up_weight,
    down_weight,
):
    tok_rows = queries_one.shape[0]
    heads_here = mix_lambda.shape[0]
    head_width = HEAD
    value_width = values.shape[1] // heads_here
    query_pos = lax.axis_index("sp") * tok_rows + jnp.arange(tok_rows, dtype=jnp.int32)
    query_first = queries_one.reshape(tok_rows, heads_here, head_width)
    query_second = queries_two.reshape(tok_rows, heads_here, head_width)
    score_scale = head_width ** (-0.5)

    def update(state, queries, key_rows, value_rows, visible):
        running, totals, weighted = state
        scores = (
            jnp.einsum("qhd,khd->hqk", queries, key_rows, preferred_element_type=jnp.float32)
            * score_scale
        )
        scores = jnp.where(visible[None], scores, masked_score)
        highest = jnp.maximum(running, jnp.max(scores, axis=2))
        weights_exp = jnp.where(visible[None], jnp.exp(scores - highest[..., None]), 0.0)
        totals = jnp.sum(weights_exp, axis=2)
        weighted = jnp.einsum(
            "hqk,khd->hqd",
            weights_exp.astype(jnp.bfloat16),
            value_rows,
            preferred_element_type=jnp.float32,
        )
        return (highest, totals, weighted)

    initial = (
        jnp.full((heads_here, tok_rows), masked_score, jnp.float32),
        jnp.zeros((heads_here, tok_rows), jnp.float32),
        jnp.zeros((heads_here, tok_rows, value_width), jnp.float32),
    )
    key_first = lax.all_gather(keys_one, "sp", axis=0, tiled=True)
    key_second = lax.all_gather(keys_two, "sp", axis=0, tiled=True)
    value_piece = lax.all_gather(values, "sp", axis=0, tiled=True)
    key_count = key_first.shape[0]
    key_pos = jnp.arange(key_count, dtype=jnp.int32)
    visible = key_pos[None, :] <= query_pos[:, None]
    value_rows = value_piece.reshape(key_count, heads_here, value_width)
    first_new = update(
        initial,
        query_first,
        key_first.reshape(key_count, heads_here, head_width),
        value_rows,
        visible,
    )
    second_new = update(
        initial,
        query_second,
        key_second.reshape(key_count, heads_here, head_width),
        value_rows,
        visible,
    )
    lam_heads = mix_lambda[:, None, None]
    mixed = (
        first_new[2] / first_new[1][..., None]
        - lam_heads * second_new[2] / second_new[1][..., None]
    )
    mean_square = jnp.mean(mixed * mixed, axis=2, keepdims=True)
    normed_heads = (
        mixed
        * lax.rsqrt(mean_square + epsilon)
        * head_gain.reshape(heads_here, 1, value_width)
        * 0.8
    )
    attended = (
        normed_heads.transpose(1, 0, 2)
        .reshape(tok_rows, heads_here * value_width)
        .astype(jnp.bfloat16)
    )
    projected = lax.psum_scatter(
        lax.dot_general(
            out_weight, attended, (((0,), (1,)), ((), ())), preferred_element_type=jnp.float32
        ).astype(jnp.bfloat16),
        "tp",
        scatter_dimension=0,
        tiled=True,
    ).astype(jnp.float32)
    resid = (residual_in.astype(jnp.float32) + projected.T).astype(jnp.bfloat16)
    full_rows = lax.all_gather(resid, "tp", axis=1, tiled=True)
    full_float = full_rows.astype(jnp.float32)
    mean_rows = jnp.mean(full_float * full_float, axis=1, keepdims=True)
    normed = (full_float * lax.rsqrt(mean_rows + epsilon) * norm_gain[None, :]).astype(jnp.bfloat16)
    gate_act = jnp.dot(
        normed,
        lax.all_gather(gate_weight, "sp", axis=0, tiled=True),
        preferred_element_type=jnp.float32,
    )
    up_act = jnp.dot(
        normed,
        lax.all_gather(up_weight, "sp", axis=0, tiled=True),
        preferred_element_type=jnp.float32,
    )
    hidden = (jax.nn.silu(gate_act) * up_act).astype(jnp.bfloat16)
    partials = jnp.dot(
        hidden,
        lax.all_gather(down_weight, "sp", axis=1, tiled=True),
        preferred_element_type=jnp.float32,
    )
    mlp_out = lax.psum_scatter(
        partials.astype(jnp.bfloat16), "tp", scatter_dimension=1, tiled=True
    ).astype(jnp.float32)
    return (resid.astype(jnp.float32) + mlp_out).astype(jnp.bfloat16)


def solution(mesh):
    in_specs = (
        P("sp", "tp"),
        P("sp", "tp"),
        P("sp", "tp"),
        P("sp", "tp"),
        P("sp", "tp"),
        P("tp"),
        P("tp"),
        P("tp", None),
        P("sp", "tp"),
        P(),
        P("sp", "tp"),
        P("sp", "tp"),
        P("tp", "sp"),
    )
    out_specs = P("sp", "tp")
    return jax.shard_map(
        per_device, mesh=mesh, in_specs=in_specs, out_specs=out_specs, check_vma=False
    )
```

profile of v0, /device:TPU:0, one launch (start us, length us, event | category | flops | bytes accessed | tf_op | source)
XLA Modules:
  0.0 449.1 jit_solution(3199958501547778345)
XLA Ops:
  6.5 0.7 all-gather.6.cloned.1.call-update
  7.3 0.0 reduce-scatter.3.cloned.1.call-start
  8.0 33.5 %all_gather.23 = bf16[2048,128]{1,0:T(8,128)(2,1)S(1)} all-gather(bf16[256,128]{1,0:T(8,128)(2,1)} %param.16), channel_id=1, replica_groups=mesh['sp'=8,'tp'=4] {'sp'}, dimensions={0}, use_global_device_ids=true | all-gather | bytes 589824 | tf_op jit(solution)/shard_map/all_gather | solution.py:59
  41.5 1.4 fusion.34
  42.9 31.7 %all_gather.21 = bf16[2048,128]{1,0:T(8,128)(2,1)S(1)} all-gather(bf16[256,128]{1,0:T(8,128)(2,1)S(1)} %copy-done.5), channel_id=1, replica_groups=mesh['sp'=8,'tp'=4] {'sp'}, dimensions={0}, use_global_device_ids=true | all-gather | bytes 589824 | tf_op jit(solution)/shard_map/all_gather | solution.py:58
  74.6 0.6 fusion.33
  75.2 1.3 copy-done.2
  76.5 1.2 fusion.9
  77.7 0.0 all-gather.6.cloned.1.call-done
  77.7 2.7 convolution_divide_fusion
  80.5 0.8 multiply_reduce_fusion
  81.4 1.5 fusion.3
  82.9 0.0 reduce-scatter.3.cloned.1.call-update
  82.9 0.0 all-gather.8.cloned.1.call-start
  83.0 26.4 %reduce-scatter.3.cloned.1.call-done = bf16[512,256]{0,1:T(8,128)(2,1)} async-done(((bf16[2048,256]{0,1:T(8,128)(2,1)}), bf16[512,256]{0,1:T(8,128)(2,1)}) %reduce-scatter.3.cloned.1.call-update) | async-done | bytes 262160 | tf_op jit(solution)/shard_map/reduce_scatter | solution.py:96
  109.4 1.7 fusion.21
  111.1 0.0 all-gather.10.cloned.1.call-start
  111.1 0.5 all-gather.10.cloned.1.call-update
  111.7 0.0 all-gather.12.cloned.1.call-start
  111.7 0.5 all-gather.12.cloned.1.call-update
  112.3 0.0 all-gather.14.cloned.1.call-start
  112.3 0.5 all-gather.14.cloned.1.call-update
  112.8 0.0 reduce-scatter.5.cloned.1.call-start
  112.9 15.1 %all-gather.8.cloned.1.call-done = bf16[256,2048]{1,0:T(8,128)(2,1)} async-done(((bf16[256,512]{1,0:T(8,128)(2,1)}), bf16[256,2048]{1,0:T(8,128)(2,1)}) %all-gather.8.cloned.1.call-update) | async-done | bytes 1048592 | tf_op jit(solution)/shard_map/all_gather | solution.py:105
  128.0 1.5 fusion.4
  129.5 92.9 %all-gather.10.cloned.1.call-done = bf16[2048,1408]{1,0:T(8,128)(2,1)} async-done(((bf16[256,1408]{1,0:T(8,128)(2,1)}), bf16[2048,1408]{1,0:T(8,128)(2,1)}) %all-gather.10.cloned.1.call-update) | async-done | bytes 5767184 | tf_op jit(solution)/shard_map/all_gather | solution.py:111
  222.4 6.0 %fusion.24 = f32[256,1408]{1,0:T(8,128)} fusion(bf16[2048,1408]{1,0:T(8,128)(2,1)} %all-gather.10.cloned.1.call-done, bf16[256,2048]{1,0:T(8,128)(2,1)} %all-gather.8.cloned.1.call-done, f32[2048]{0:T(1024)S(1)} %copy-done.9, f32[256]{0:T(256)S(1)} %add_rsqrt_fusion), kind=kOutput, calls=%fused_computation.34 | convolution fusion | flops 1478492160 | bytes 8266752 | tf_op jit(solution)/shard_map/dot_general | solution.py:109
  228.3 86.6 %all-gather.12.cloned.1.call-done = bf16[2048,1408]{1,0:T(8,128)(2,1)} async-done(((bf16[256,1408]{1,0:T(8,128)(2,1)}), bf16[2048,1408]{1,0:T(8,128)(2,1)}) %all-gather.12.cloned.1.call-update) | async-done | bytes 5767184 | tf_op jit(solution)/shard_map/all_gather | solution.py:116
  314.9 93.2 %all-gather.14.cloned.1.call-done = bf16[1408,2048]{1,0:T(8,128)(2,1)} async-done(((bf16[1408,256]{1,0:T(8,128)(2,1)}), bf16[1408,2048]{1,0:T(8,128)(2,1)}) %all-gather.14.cloned.1.call-update) | async-done | bytes 5767184 | tf_op jit(solution)/shard_map/all_gather | solution.py:122
  408.2 9.3 %convolution_convert_fusion.1 = bf16[256,2048]{1,0:T(8,128)(2,1)} fusion(bf16[1408,2048]{1,0:T(8,128)(2,1)} %all-gather.14.cloned.1.call-done, bf16[2048,1408]{1,0:T(8,128)(2,1)} %all-gather.12.cloned.1.call-done, f32[256,1408]{1,0:T(8,128)} %fusion.24, bf16[256,2048]{1,0:T(8,128)(2,1)S(1)} %copy-done.3, f32[2048]{0:T(1024)S(1)} %copy-done.9, ...), kind=kOutput, calls=%fused_computation.9 | convolution fusion | flops 2957574144 | bytes 15082496 | tf_op jit(solution)/shard_map/dot_general | solution.py:120
  417.4 23.1 %reduce-scatter.5.cloned.1.call-done = bf16[256,512]{1,0:T(8,128)(2,1)} async-done(((bf16[256,2048]{1,0:T(8,128)(2,1)}), bf16[256,512]{1,0:T(8,128)(2,1)}) %reduce-scatter.5.cloned.1.call-update) | async-done | bytes 262160 | tf_op jit(solution)/shard_map/reduce_scatter | solution.py:125
  440.6 1.7 add_convert_fusion
  (27 shorter events, 0.1 us)
Async XLA Ops:
  6.5 74.8 %copy-start = (bf16[256,2048]{1,0:T(8,128)(2,1)S(1)}, bf16[256,2048]{1,0:T(8,128)(2,1)}, u32[]{:S(2)}) copy-start(bf16[256,2048]{1,0:T(8,128)(2,1)} %param.20) | copy-start | bytes 3145732
  6.5 36.4 %copy-start.5 = (bf16[256,128]{1,0:T(8,128)(2,1)S(1)}, bf16[256,128]{1,0:T(8,128)(2,1)}, u32[]{:S(2)}) copy-start(bf16[256,128]{1,0:T(8,128)(2,1)} %param.15) | copy-start | bytes 196612
  6.5 68.1 %copy-start.8 = (bf16[256,128]{1,0:T(8,128)(2,1)S(1)}, bf16[256,128]{1,0:T(8,128)(2,1)}, u32[]{:S(2)}) copy-start(bf16[256,128]{1,0:T(8,128)(2,1)} %param.13) | copy-start | bytes 196612
  6.5 71.2 %all-gather.6.cloned.1.call-start = ((), (), s32[]{:S(2)}) async-start(), calls=%async_computation.2 | async-start | bytes 1179648 | tf_op jit(solution)/shard_map/all_gather | solution.py:60
  7.3 102.1 %reduce-scatter.3.cloned.1.call-start = ((), (), s32[]{:S(2)}) async-start(), calls=%async_computation.3 | async-start | bytes 1310720 | tf_op jit(solution)/shard_map/reduce_scatter | solution.py:96
  75.2 1.3 copy-start.2
  77.7 2.7 copy-start.7
  80.5 0.9 copy-start.6
  81.3 28.1 %copy-start.4 = (bf16[256,512]{1,0:T(8,128)(2,1)S(1)}, bf16[256,512]{1,0:T(8,128)(2,1)}, u32[]{:S(2)}) copy-start(bf16[256,512]{1,0:T(8,128)(2,1)} %param.21) | copy-start | bytes 786436
  82.9 139.5 %copy-start.9 = (f32[2048]{0:T(1024)S(1)}, f32[2048]{0:T(1024)}, u32[]{:S(2)}) copy-start(f32[2048]{0:T(1024)} %param.22) | copy-start | bytes 24580
  82.9 45.1 %all-gather.8.cloned.1.call-start = ((), (), s32[]{:S(2)}) async-start(), calls=%async_computation.4 | async-start | bytes 1310720 | tf_op jit(solution)/shard_map/all_gather | solution.py:105
  111.1 111.3 %all-gather.10.cloned.1.call-start = ((), (), s32[]{:S(2)}) async-start(), calls=%async_computation.5 | async-start | bytes 6488064 | tf_op jit(solution)/shard_map/all_gather | solution.py:111
  111.7 203.2 %all-gather.12.cloned.1.call-start = ((), (), s32[]{:S(2)}) async-start(), calls=%async_computation.6 | async-start | bytes 6488064 | tf_op jit(solution)/shard_map/all_gather | solution.py:116
  112.3 295.9 %all-gather.14.cloned.1.call-start = ((), (), s32[]{:S(2)}) async-start(), calls=%async_computation.7 | async-start | bytes 6488064 | tf_op jit(solution)/shard_map/all_gather | solution.py:122
  112.8 327.7 %reduce-scatter.5.cloned.1.call-start = ((), (), s32[]{:S(2)}) async-start(), calls=%async_computation.8 | async-start | bytes 1310720 | tf_op jit(solution)/shard_map/reduce_scatter | solution.py:125
  129.5 278.7 %copy-start.3 = (bf16[256,2048]{1,0:T(8,128)(2,1)S(1)}, bf16[256,2048]{1,0:T(8,128)(2,1)}, u32[]{:S(2)}) copy-start(bf16[256,2048]{1,0:T(8,128)(2,1)} %all-gather.8.cloned.1.call-done) | copy-start | bytes 3145732
  228.3 212.3 %copy-start.1 = (bf16[256,512]{1,0:T(8,128)(2,1)S(1)}, bf16[256,512]{1,0:T(8,128)(2,1)}, u32[]{:S(2)}) copy-start(bf16[256,512]{1,0:T(8,128)(2,1)} %fusion.21) | copy-start | bytes 786436
Sparse Core Ops, SparseCore 0:
  9.5 44.7 all-gather.5
  83.0 26.2 reduce-scatter.2
  111.2 16.7 all-gather.7
  130.0 92.3 all-gather.9
  224.4 90.4 all-gather.11
  316.8 91.2 all-gather.13
  417.6 22.9 reduce-scatter.4
where the time goes:
time: 449 us
  waiting for transfers between devices  340 us (76%)
  blocking collectives  65.2 us (15%)
  matrix products  22.3 us (5%)
  between operations  14.3 us (3%)
  other arithmetic  6.13 us (1%)
    all_gather x1, waiting for transfers between devices, per_device(): lax.all_gather(down_weight, 'sp', axis=1, tiled=True)  93.2 us
    all_gather x1, waiting for transfers between devices, per_device(): lax.all_gather(gate_weight, 'sp', axis=0, tiled=True)  92.9 us
    all_gather x1, waiting for transfers between devices, per_device(): lax.all_gather(up_weight, 'sp', axis=0, tiled=True)  86.6 us
    all_gather x1, blocking collectives, per_device(): key_second = lax.all_gather(keys_two, 'sp', axis=0, tiled=True)  33.5 us
    all_gather x1, blocking collectives, per_device(): key_first = lax.all_gather(keys_one, 'sp', axis=0, tiled=True)  31.7 us
    reduce_scatter x1, waiting for transfers between devices, per_device(): lax.psum_scatter(lax.dot_general(out_weight, attended, (((0,), (1,)), (()...  26.4 us
    reduce_scatter x1, waiting for transfers between devices, per_device(): lax.psum_scatter(partials.astype(jnp.bfloat16), 'tp', scatter_dimension=1...  23.1 us
    all_gather x1, waiting for transfers between devices, per_device(): full_rows = lax.all_gather(resid, 'tp', axis=1, tiled=True)  15.1 us
  transfers between devices with their start and end apart: 7, of which 6 were waited for; matrix products, arithmetic and copies ran while one was open for 2% of the time, Pallas kernels for 0%

commit v1 on v0

--- a/solution.py
+++ b/solution.py
@@ -56,7 +56,15 @@
         jnp.zeros((heads_here, tok_rows, value_width), jnp.float32),
     )
     key_first = lax.all_gather(keys_one, "sp", axis=0, tiled=True)
-    key_second = lax.all_gather(keys_two, "sp", axis=0, tiled=True)
+    sides = jax.lax.axis_size("sp")
+    samples = [(at, (at + 1) % sides) for at in range(sides)]
+    u_next = [None] * sides
+    u_next[sides - 1] = keys_two
+    for to_i in range(sides - 2, -1, -1):
+        u_next[to_i] = jax.lax.ppermute(u_next[to_i + 1], "sp", samples)
+    key_second = jnp.roll(
+        jnp.concatenate(u_next, axis=0), (jax.lax.axis_index("sp") + 1) * keys_two.shape[0], axis=0
+    )
     value_piece = lax.all_gather(values, "sp", axis=0, tiled=True)
     key_count = key_first.shape[0]
     key_pos = jnp.arange(key_count, dtype=jnp.int32)

time: 449 us -> 459 us (1.022)
  waiting for transfers between devices: 340 us -> 372 us
  blocking collectives: 65.2 us -> 34.3 us
  starting transfers between devices: 0.24 us -> 5.05 us
    ppermute x0 -> x7, waiting for transfers between devices: none -> 36.5 us  [per_device(): u_next[to_i] = jax.lax.ppermute(u_next[to_i + 1], 'sp', samples)]
    all_gather x1 -> x0, blocking collectives: 33.5 us -> none  [per_device(): key_second = lax.all_gather(keys_two, 'sp', axis=0, tiled=True)]
    ppermute x0 -> x7, starting transfers between devices: none -> 4.81 us  [per_device(): u_next[to_i] = jax.lax.ppermute(u_next[to_i + 1], 'sp', samples)]
  transfers between devices with their start and end apart: 7 -> 14, of which waited for: 6 -> 12; matrix products, arithmetic and copies ran while one was open for 2% -> 3% of each run, Pallas kernels for 0% -> 0%
where the time goes in v1:
time: 459 us; the launch traced here: 458 us
  waiting for transfers between devices  372 us (81%)
  blocking collectives  34.3 us (7%)
  matrix products  22 us (5%)
  between operations  14.4 us (3%)
  other arithmetic  6.11 us (1%)
  starting transfers between devices  5.05 us (1%)
  local copies, waits for them, and re-layouts  4.95 us (1%)
    all_gather x1, waiting for transfers between devices, per_device(): lax.all_gather(down_weight, 'sp', axis=1, tiled=True)  93.2 us
    all_gather x1, waiting for transfers between devices, per_device(): lax.all_gather(gate_weight, 'sp', axis=0, tiled=True)  92.9 us
    all_gather x1, waiting for transfers between devices, per_device(): lax.all_gather(up_weight, 'sp', axis=0, tiled=True)  86.6 us
    ppermute x7, waiting for transfers between devices, per_device(): u_next[to_i] = jax.lax.ppermute(u_next[to_i + 1], 'sp', samples)  36.5 us
    all_gather x1, blocking collectives, per_device(): key_first = lax.all_gather(keys_one, 'sp', axis=0, tiled=True)  34.3 us
    reduce_scatter x1, waiting for transfers between devices, per_device(): lax.psum_scatter(partials.astype(jnp.bfloat16), 'tp', scatter_dimension=1...  23.1 us
    reduce_scatter x1, waiting for transfers between devices, per_device(): lax.psum_scatter(lax.dot_general(out_weight, attended, (((0,), (1,)), (()...  22.5 us
    all_gather x1, waiting for transfers between devices, per_device(): full_rows = lax.all_gather(resid, 'tp', axis=1, tiled=True)  15.1 us
  transfers between devices with their start and end apart: 14, of which 12 were waited for; matrix products, arithmetic and copies ran while one was open for 3% of the time, Pallas kernels for 0%

profile of v1, /device:TPU:0, one launch (start us, length us, event | category | flops | bytes accessed | tf_op | source)
XLA Modules:
  0.0 458.3 jit_solution(8237977308402639834)
XLA Ops:
  6.5 3.0 collective-permute-start
  9.5 5.5 %collective-permute-done = bf16[256,128]{1,0:T(8,128)(2,1)S(1)} collective-permute-done((bf16[256,128]{1,0:T(8,128)(2,1)}, bf16[256,128]{1,0:T(8,128)(2,1)S(1)}, u32[]{:S(2)}, u32[]{:S(2)}) %collective-permute-start) | collective-permute-done | bytes 65568 | tf_op jit(solution)/shard_map/ppermute | solution.py:64
  15.0 7.0 %collective-permute-done.1 = bf16[256,128]{1,0:T(8,128)(2,1)S(1)} collective-permute-done((bf16[256,128]{1,0:T(8,128)(2,1)S(1)}, bf16[256,128]{1,0:T(8,128)(2,1)S(1)}, u32[]{:S(2)}, u32[]{:S(2)}) %collective-permute-start.1) | collective-permute-done | bytes 65568 | tf_op jit(solution)/shard_map/ppermute | solution.py:64
  22.0 7.0 %collective-permute-done.2 = bf16[256,128]{1,0:T(8,128)(2,1)S(1)} collective-permute-done((bf16[256,128]{1,0:T(8,128)(2,1)S(1)}, bf16[256,128]{1,0:T(8,128)(2,1)S(1)}, u32[]{:S(2)}, u32[]{:S(2)}) %collective-permute-start.2) | collective-permute-done | bytes 65568 | tf_op jit(solution)/shard_map/ppermute | solution.py:64
  29.0 6.9 %collective-permute-done.3 = bf16[256,128]{1,0:T(8,128)(2,1)S(1)} collective-permute-done((bf16[256,128]{1,0:T(8,128)(2,1)S(1)}, bf16[256,128]{1,0:T(8,128)(2,1)S(1)}, u32[]{:S(2)}, u32[]{:S(2)}) %collective-permute-start.3) | collective-permute-done | bytes 65568 | tf_op jit(solution)/shard_map/ppermute | solution.py:64
  35.9 34.3 %all_gather.18 = bf16[2048,128]{1,0:T(8,128)(2,1)} all-gather(bf16[256,128]{1,0:T(8,128)(2,1)} %param.15), channel_id=1, replica_groups=mesh['sp'=8,'tp'=4] {'sp'}, dimensions={0}, use_global_device_ids=true | all-gather | bytes 589824 | tf_op jit(solution)/shard_map/all_gather | solution.py:58
  70.2 1.8 collective-permute-start.5
  72.0 5.3 %collective-permute-done.5 = bf16[256,128]{1,0:T(8,128)(2,1)} collective-permute-done((bf16[256,128]{1,0:T(8,128)(2,1)S(1)}, bf16[256,128]{1,0:T(8,128)(2,1)}, u32[]{:S(2)}, u32[]{:S(2)}) %collective-permute-start.5) | collective-permute-done | bytes 65568 | tf_op jit(solution)/shard_map/ppermute | solution.py:64
  77.3 1.7 fusion.36
  79.6 4.9 %collective-permute-done.6 = bf16[256,128]{1,0:T(8,128)(2,1)} collective-permute-done((bf16[256,128]{1,0:T(8,128)(2,1)}, bf16[256,128]{1,0:T(8,128)(2,1)}, u32[]{:S(2)}, u32[]{:S(2)}) %collective-permute-start.6) | collective-permute-done | bytes 65568 | tf_op jit(solution)/shard_map/ppermute | solution.py:64
  84.6 0.8 constant_dynamic-update-slice_fusion.15
  85.4 0.9 constant_dynamic-update-slice_fusion.14
  86.4 0.9 constant_dynamic-update-slice_fusion.7
  87.3 0.9 constant_dynamic-update-slice_fusion.6
  88.2 0.6 fusion.37
  88.8 1.3 copy-done.2
  90.2 1.1 fusion.10
  91.4 2.2 convolution_divide_fusion
  93.5 0.8 multiply_reduce_fusion
  94.4 1.5 fusion.4
  96.0 22.5 %reduce-scatter.3.cloned.1.call-done = bf16[512,256]{0,1:T(8,128)(2,1)} async-done(((bf16[2048,256]{0,1:T(8,128)(2,1)}), bf16[512,256]{0,1:T(8,128)(2,1)}) %reduce-scatter.3.cloned.1.call-update) | async-done | bytes 262160 | tf_op jit(solution)/shard_map/reduce_scatter | solution.py:104
  118.5 1.7 fusion.22
  120.9 0.5 all-gather.12.cloned.1.call-update
  122.0 15.1 %all-gather.8.cloned.1.call-done = bf16[256,2048]{1,0:T(8,128)(2,1)} async-done(((bf16[256,512]{1,0:T(8,128)(2,1)}), bf16[256,2048]{1,0:T(8,128)(2,1)}) %all-gather.8.cloned.1.call-update) | async-done | bytes 1048592 | tf_op jit(solution)/shard_map/all_gather | solution.py:113
  137.1 1.5 fusion.5
  138.6 92.9 %all-gather.10.cloned.1.call-done = bf16[2048,1408]{1,0:T(8,128)(2,1)} async-done(((bf16[256,1408]{1,0:T(8,128)(2,1)}), bf16[2048,1408]{1,0:T(8,128)(2,1)}) %all-gather.10.cloned.1.call-update) | async-done | bytes 5767184 | tf_op jit(solution)/shard_map/all_gather | solution.py:119
  231.5 6.0 %fusion.26 = f32[256,1408]{1,0:T(8,128)} fusion(bf16[2048,1408]{1,0:T(8,128)(2,1)} %all-gather.10.cloned.1.call-done, bf16[256,2048]{1,0:T(8,128)(2,1)} %all-gather.8.cloned.1.call-done, f32[2048]{0:T(1024)S(1)} %copy-done.10, f32[256]{0:T(256)S(1)} %add_rsqrt_fusion), kind=kOutput, calls=%fused_computation.36 | convolution fusion | flops 1478492160 | bytes 8266752 | tf_op jit(solution)/shard_map/dot_general | solution.py:117
  237.5 86.6 %all-gather.12.cloned.1.call-done = bf16[2048,1408]{1,0:T(8,128)(2,1)} async-done(((bf16[256,1408]{1,0:T(8,128)(2,1)}), bf16[2048,1408]{1,0:T(8,128)(2,1)}) %all-gather.12.cloned.1.call-update) | async-done | bytes 5767184 | tf_op jit(solution)/shard_map/all_gather | solution.py:124
  324.1 93.2 %all-gather.14.cloned.1.call-done = bf16[1408,2048]{1,0:T(8,128)(2,1)} async-done(((bf16[1408,256]{1,0:T(8,128)(2,1)}), bf16[1408,2048]{1,0:T(8,128)(2,1)}) %all-gather.14.cloned.1.call-update) | async-done | bytes 5767184 | tf_op jit(solution)/shard_map/all_gather | solution.py:130
  417.3 9.3 %convolution_convert_fusion.1 = bf16[256,2048]{1,0:T(8,128)(2,1)} fusion(bf16[1408,2048]{1,0:T(8,128)(2,1)} %all-gather.14.cloned.1.call-done, bf16[2048,1408]{1,0:T(8,128)(2,1)} %all-gather.12.cloned.1.call-done, f32[256,1408]{1,0:T(8,128)} %fusion.26, bf16[256,2048]{1,0:T(8,128)(2,1)S(1)} %copy-done.4, f32[2048]{0:T(1024)S(1)} %copy-done.10, ...), kind=kOutput, calls=%fused_computation.10 | convolution fusion | flops 2957574144 | bytes 15082496 | tf_op jit(solution)/shard_map/dot_general | solution.py:128
  426.6 23.1 %reduce-scatter.5.cloned.1.call-done = bf16[256,512]{1,0:T(8,128)(2,1)} async-done(((bf16[256,2048]{1,0:T(8,128)(2,1)}), bf16[256,512]{1,0:T(8,128)(2,1)}) %reduce-scatter.5.cloned.1.call-update) | async-done | bytes 262160 | tf_op jit(solution)/shard_map/reduce_scatter | solution.py:133
  449.7 1.7 add_convert_fusion
  (57 shorter events, 1.6 us)
Async XLA Ops:
  6.5 87.9 %copy-start = (bf16[256,2048]{1,0:T(8,128)(2,1)S(1)}, bf16[256,2048]{1,0:T(8,128)(2,1)}, u32[]{:S(2)}) copy-start(bf16[256,2048]{1,0:T(8,128)(2,1)} %param.20) | copy-start | bytes 3145732
  6.5 84.8 %all-gather.6.cloned.1.call-start = ((), (), s32[]{:S(2)}) async-start(), calls=%async_computation.2 | async-start | bytes 1179648 | tf_op jit(solution)/shard_map/all_gather | solution.py:68
  6.5 8.5 %collective-permute-start = (bf16[256,128]{1,0:T(8,128)(2,1)}, bf16[256,128]{1,0:T(8,128)(2,1)S(1)}, u32[]{:S(2)}, u32[]{:S(2)}) collective-permute-start(bf16[256,128]{1,0:T(8,128)(2,1)} %param.16), channel_id=1, source_target_pairs={{0,4},{4,8},{8,12},{12,16},{16,20},{20,24},{24,28},{28,0},{1,5},{5... | collective-permute-start | bytes 196616 | tf_op jit(solution)/shard_map/ppermute | solution.py:64
  15.0 7.0 %collective-permute-start.1 = (bf16[256,128]{1,0:T(8,128)(2,1)S(1)}, bf16[256,128]{1,0:T(8,128)(2,1)S(1)}, u32[]{:S(2)}, u32[]{:S(2)}) collective-permute-start(bf16[256,128]{1,0:T(8,128)(2,1)S(1)} %collective-permute-done), channel_id=1, source_target_pairs={{0,4},{4,8},{8,12},{12,16},{16,20},{20,24},{24,28},{28,0},{1,5},{5... | collective-permute-start | bytes 196616 | tf_op jit(solution)/shard_map/ppermute | solution.py:64
  22.0 7.0 %collective-permute-start.2 = (bf16[256,128]{1,0:T(8,128)(2,1)S(1)}, bf16[256,128]{1,0:T(8,128)(2,1)S(1)}, u32[]{:S(2)}, u32[]{:S(2)}) collective-permute-start(bf16[256,128]{1,0:T(8,128)(2,1)S(1)} %collective-permute-done.1), channel_id=1, source_target_pairs={{0,4},{4,8},{8,12},{12,16},{16,20},{20,24},{24,28},{28,0},{1,5},{5... | collective-permute-start | bytes 196616 | tf_op jit(solution)/shard_map/ppermute | solution.py:64
  29.0 7.0 %collective-permute-start.3 = (bf16[256,128]{1,0:T(8,128)(2,1)S(1)}, bf16[256,128]{1,0:T(8,128)(2,1)S(1)}, u32[]{:S(2)}, u32[]{:S(2)}) collective-permute-start(bf16[256,128]{1,0:T(8,128)(2,1)S(1)} %collective-permute-done.2), channel_id=1, source_target_pairs={{0,4},{4,8},{8,12},{12,16},{16,20},{20,24},{24,28},{28,0},{1,5},{5... | collective-permute-start | bytes 196616 | tf_op jit(solution)/shard_map/ppermute | solution.py:64
  29.0 57.4 %copy-start.6 = (bf16[256,128]{1,0:T(8,128)(2,1)S(1)}, bf16[256,128]{1,0:T(8,128)(2,1)}, u32[]{:S(2)}) copy-start(bf16[256,128]{1,0:T(8,128)(2,1)} %param.16) | copy-start | bytes 196612
  29.0 89.5 %reduce-scatter.3.cloned.1.call-start = ((), (), s32[]{:S(2)}) async-start(), calls=%async_computation.3 | async-start | bytes 1310720 | tf_op jit(solution)/shard_map/reduce_scatter | solution.py:104
  35.9 34.3 %collective-permute-start.4 = (bf16[256,128]{1,0:T(8,128)(2,1)S(1)}, bf16[256,128]{1,0:T(8,128)(2,1)S(1)}, u32[]{:S(2)}, u32[]{:S(2)}) collective-permute-start(bf16[256,128]{1,0:T(8,128)(2,1)S(1)} %collective-permute-done.3), channel_id=1, source_target_pairs={{0,4},{4,8},{8,12},{12,16},{16,20},{20,24},{24,28},{28,0},{1,5},{5... | collective-permute-start | bytes 196616 | tf_op jit(solution)/shard_map/ppermute | solution.py:64
  70.2 7.1 %collective-permute-start.5 = (bf16[256,128]{1,0:T(8,128)(2,1)S(1)}, bf16[256,128]{1,0:T(8,128)(2,1)}, u32[]{:S(2)}, u32[]{:S(2)}) collective-permute-start(bf16[256,128]{1,0:T(8,128)(2,1)S(1)} %collective-permute-done.4), channel_id=1, source_target_pairs={{0,4},{4,8},{8,12},{12,16},{16,20},{20,24},{24,28},{28,0},{1,5},{5... | collective-permute-start | bytes 196616 | tf_op jit(solution)/shard_map/ppermute | solution.py:64
  77.3 7.3 %collective-permute-start.6 = (bf16[256,128]{1,0:T(8,128)(2,1)}, bf16[256,128]{1,0:T(8,128)(2,1)}, u32[]{:S(2)}, u32[]{:S(2)}) collective-permute-start(bf16[256,128]{1,0:T(8,128)(2,1)} %collective-permute-done.5), channel_id=1, source_target_pairs={{0,4},{4,8},{8,12},{12,16},{16,20},{20,24},{24,28},{28,0},{1,5},{5... | collective-permute-start | bytes 196616 | tf_op jit(solution)/shard_map/ppermute | solution.py:64
  79.6 8.6 %copy-start.9 = (bf16[256,128]{1,0:T(8,128)(2,1)S(1)}, bf16[256,128]{1,0:T(8,128)(2,1)}, u32[]{:S(2)}) copy-start(bf16[256,128]{1,0:T(8,128)(2,1)} %param.14) | copy-start | bytes 196612
  88.8 1.3 copy-start.2
  91.3 2.2 copy-start.3
  91.3 2.2 copy-start.8
  93.5 0.9 copy-start.7
  94.4 24.1 %copy-start.5 = (bf16[256,512]{1,0:T(8,128)(2,1)S(1)}, bf16[256,512]{1,0:T(8,128)(2,1)}, u32[]{:S(2)}) copy-start(bf16[256,512]{1,0:T(8,128)(2,1)} %param.21) | copy-start | bytes 786436
  96.0 135.5 %copy-start.10 = (f32[2048]{0:T(1024)S(1)}, f32[2048]{0:T(1024)}, u32[]{:S(2)}) copy-start(f32[2048]{0:T(1024)} %param.22) | copy-start | bytes 24580
  96.0 41.1 %all-gather.8.cloned.1.call-start = ((), (), s32[]{:S(2)}) async-start(), calls=%async_computation.4 | async-start | bytes 1310720 | tf_op jit(solution)/shard_map/all_gather | solution.py:113
  120.3 111.2 %all-gather.10.cloned.1.call-start = ((), (), s32[]{:S(2)}) async-start(), calls=%async_computation.5 | async-start | bytes 6488064 | tf_op jit(solution)/shard_map/all_gather | solution.py:119
  120.8 203.2 %all-gather.12.cloned.1.call-start = ((), (), s32[]{:S(2)}) async-start(), calls=%async_computation.6 | async-start | bytes 6488064 | tf_op jit(solution)/shard_map/all_gather | solution.py:124
  121.4 295.9 %all-gather.14.cloned.1.call-start = ((), (), s32[]{:S(2)}) async-start(), calls=%async_computation.7 | async-start | bytes 6488064 | tf_op jit(solution)/shard_map/all_gather | solution.py:130
  122.0 327.7 %reduce-scatter.5.cloned.1.call-start = ((), (), s32[]{:S(2)}) async-start(), calls=%async_computation.8 | async-start | bytes 1310720 | tf_op jit(solution)/shard_map/reduce_scatter | solution.py:133
  138.6 278.7 %copy-start.4 = (bf16[256,2048]{1,0:T(8,128)(2,1)S(1)}, bf16[256,2048]{1,0:T(8,128)(2,1)}, u32[]{:S(2)}) copy-start(bf16[256,2048]{1,0:T(8,128)(2,1)} %all-gather.8.cloned.1.call-done) | copy-start | bytes 3145732
  237.5 212.3 %copy-start.1 = (bf16[256,512]{1,0:T(8,128)(2,1)S(1)}, bf16[256,512]{1,0:T(8,128)(2,1)}, u32[]{:S(2)}) copy-start(bf16[256,512]{1,0:T(8,128)(2,1)} %fusion.22) | copy-start | bytes 786436
Sparse Core Ops, SparseCore 0:
  29.1 44.1 all-gather.5
  96.1 22.3 reduce-scatter.2
  120.4 16.6 all-gather.7
  139.2 92.3 all-gather.9
  233.5 90.4 all-gather.11
  326.0 91.2 all-gather.13
  426.7 22.9 reduce-scatter.4
